TPU v7x, 32 devices: a whole 2x2x4 slice. The times are simulated.
32 devices in a mesh: fs: 8 (over z, x), tp: 4 (over y, core).
Axes of the slice: x: 2, y: 2, z: 4, core: 2. Of those that a mesh axis runs over, the one named last changes fastest.
Arguments:
- tokens: bfloat16 [8192, 2048], P(('fs', 'tp')), may hold values from -6 to 6
- gate_pre: bfloat16 [8192, 5632], P('fs', 'tp'), may hold values from -6 to 6
- value_pre: bfloat16 [8192, 5632], P('fs', 'tp'), may hold values from -6 to 6
- up_gate_w: bfloat16 [2048, 5632], P('fs', 'tp'), may hold values from -0.078125 to 0.078125
- up_value_w: bfloat16 [2048, 5632], P('fs', 'tp'), may hold values from -0.078125 to 0.078125
- conv_weight: float32 [3, 5632], P(None, 'tp'), may hold values from -3 to 3
- conv_bias: float32 [5632], P('tp'), may hold values from -3 to 3
- hidden_grad: bfloat16 [8192, 5632], P('fs', 'tp'), may hold values from -6 to 6
Outputs:
- input_grad: bfloat16 [8192, 2048], P(('fs', 'tp'))
- up_gate_grad: float32 [2048, 5632], P('fs', 'tp')
- up_value_grad: float32 [2048, 5632], P('fs', 'tp')
- conv_weight_grad: float32 [3, 5632], P(None, 'tp')
- conv_bias_grad: float32 [5632], P('tp')
All inputs are finite; a program needn't handle non-finite values.
Results may differ from a plain program's by a relative error of at most 0.013.
Values may be sent and summed in bfloat16 or wider, within the bound.
A program may use at most 128 MiB of HBM per device.

v0:
```python
import jax
import jax.numpy as jnp
from jax import lax
from jax.sharding import PartitionSpec as P


def contract_rows(left, right):
    return lax.dot_general(
        left, right, (((0,), (0,)), ((), ())), preferred_element_type=jnp.float32
    )


def contract_cols(left, right):
    return lax.dot_general(
        left, right, (((1,), (1,)), ((), ())), preferred_element_type=jnp.float32
    )


def on_device(
    tokens, gate_pre, value_pre, up_gate_w, up_value_w, conv_weight, conv_bias, hidden_grad
):
    length = gate_pre.shape[0]
    col_count = gate_pre.shape[1]
    scale = float(length * lax.axis_size("fs")) ** (-0.5)
    gate_float = gate_pre.astype(jnp.float32)
    padded = jnp.pad(gate_float, ((2, 0), (0, 0)))
    gate_conv = (
        conv_bias
        + conv_weight[0] * padded[:length]
        + conv_weight[1] * padded[1 : length + 1]
        + conv_weight[2] * padded[2:]
    )
    active, gelu_back = jax.vjp(jax.nn.gelu, gate_conv)
    grad_float = hidden_grad.astype(jnp.float32)
    value_grad = (grad_float * active).astype(jnp.bfloat16)
    conv_grad = gelu_back(grad_float * value_pre.astype(jnp.float32))[0]
    shifted = jnp.pad(conv_grad, ((0, 2), (0, 0)))
    gate_grad = (
        conv_weight[2] * conv_grad
        + conv_weight[1] * shifted[1 : length + 1]
        + conv_weight[0] * shifted[2:]
    ).astype(jnp.bfloat16)
    conv_terms = jnp.stack(
        [
            jnp.sum(conv_grad * padded[:length], axis=0),
            jnp.sum(conv_grad * padded[1 : length + 1], axis=0),
            jnp.sum(conv_grad * padded[2:], axis=0),
            jnp.sum(conv_grad, axis=0),
        ]
    )
    conv_total = lax.psum(conv_terms, "fs") * scale
    whole_tokens = lax.all_gather(tokens, "tp", axis=0, tiled=True)
    full_gate, full_value = (
        lax.all_gather(up_gate_w, "fs", axis=0, tiled=True),
        lax.all_gather(up_value_w, "fs", axis=0, tiled=True),
    )
    joined = lax.psum_scatter(
        jnp.concatenate(
            [contract_rows(whole_tokens, gate_grad), contract_rows(whole_tokens, value_grad)],
            axis=1,
        ),
        "fs",
        scatter_dimension=0,
        tiled=True,
    )
    gate_out = joined[:, :col_count] * scale
    value_out = joined[:, col_count:] * scale
    input_grad = lax.psum_scatter(
        (contract_cols(gate_grad, full_gate) + contract_cols(value_grad, full_value)).astype(
            jnp.bfloat16
        ),
        "tp",
        scatter_dimension=0,
        tiled=True,
    )
    return (input_grad, gate_out, value_out, conv_total[:3], conv_total[3])


def solution(mesh):
    return jax.shard_map(
        on_device,
        mesh=mesh,
        in_specs=(
            P(("fs", "tp"), None),
            P("fs", "tp"),
            P("fs", "tp"),
            P("fs", "tp"),
            P("fs", "tp"),
            P(None, "tp"),
            P("tp"),
            P("fs", "tp"),
        ),
        out_specs=(P(("fs", "tp"), None), P("fs", "tp"), P("fs", "tp"), P(None, "tp"), P("tp")),
        check_vma=False,
    )
```

profile of v0, /device:TPU:0, one launch (start us, length us, event | category | flops | bytes accessed | tf_op | source)
XLA Modules:
  0.0 663.5 jit_solution(3826145248827536380)
XLA Ops:
  7.2 0.7 all-gather.8.cloned.1.call-update
  8.0 0.7 all-gather.4.cloned.1.call-update
  8.7 0.7 all-gather.6.cloned.1.call-update
  9.5 2.3 convert_element_type.24
  11.9 0.2 copy-done.1
  12.1 0.9 copy-done.2
  13.0 9.3 %multiply_reduce_fusion.2 = (f32[1408]{0:T(1024)S(1)}, f32[1408]{0:T(1024)S(1)}, f32[1408]{0:T(1024)S(1)}, f32[1408]{0:T(1024)S(1)}, f32[1024,1408]{1,0:T(8,128)S(1)}, /*index=5*/f32[1024,1408]{1,0:T(8,128)}) fusion(f32[1024,1408]{1,0:T(8,128)S(1)} %convert_element_type.24, bf16[1024,1408]{1,0:T(8,128)(2,1)S(1)} %copy-done, ...), kind=kLoop, calls=%fused_computation.17 | loop fusion | flops 51898880 | bytes 25997312 | tf_op jit(solution)/shard_map/reduce_sum | solution.py:45
  22.3 3.0 add_convert_fusion.1
  25.3 21.5 %all-gather.8.cloned.1.call-done = bf16[1024,2048]{1,0:T(8,128)(2,1)} async-done(((bf16[256,2048]{1,0:T(8,128)(2,1)}), bf16[1024,2048]{1,0:T(8,128)(2,1)}) %all-gather.8.cloned.1.call-update) | async-done | bytes 4194320 | tf_op jit(solution)/shard_map/all_gather | solution.py:52
  46.8 12.8 %convolution_bitcast_fusion = f32[2048,1408]{0,1:T(8,128)S(1)} fusion(bf16[1024,2048]{1,0:T(8,128)(2,1)} %all-gather.8.cloned.1.call-done, bf16[1024,1408]{1,0:T(8,128)(2,1)S(1)} %copy-done.3, f32[1024,1408]{1,0:T(8,128)} %get-tuple-element.18), kind=kOutput, calls=%fused_computation.1 | convolution fusion | flops 5921439744 | bytes 24379392 | tf_op jit(solution)/shard_map/dot_general | solution.py:8
  59.6 9.0 %convolution_bitcast_fusion.1 = f32[2048,1408]{0,1:T(8,128)S(1)} fusion(bf16[1024,1408]{1,0:T(8,128)(2,1)} %add_convert_fusion.1, bf16[1024,2048]{1,0:T(8,128)(2,1)} %all-gather.8.cloned.1.call-done), kind=kOutput, calls=%fused_computation.2 | convolution fusion | flops 5905580032 | bytes 18612224 | tf_op jit(solution)/shard_map/dot_general | solution.py:8
  68.5 11.3 %pad_maximum_fusion = f32[2048,2816]{0,1:T(8,128)} fusion(f32[2048,1408]{0,1:T(8,128)S(1)} %convolution_bitcast_fusion, f32[2048,1408]{0,1:T(8,128)S(1)} %convolution_bitcast_fusion.1), kind=kLoop, calls=%fused_computation | loop fusion | flops 5767168 | bytes 46137344 | tf_op jit(solution)/shard_map/concatenate | solution.py:58
  79.8 0.2 reduce-scatter.3.cloned.1.call-start
  80.1 61.2 %all-gather.4.cloned.1.call-done = bf16[2048,1408]{1,0:T(8,128)(2,1)} async-done(((bf16[256,1408]{1,0:T(8,128)(2,1)}), bf16[2048,1408]{1,0:T(8,128)(2,1)}) %all-gather.4.cloned.1.call-update) | async-done | bytes 5767184 | tf_op jit(solution)/shard_map/all_gather | solution.py:54
  141.3 11.6 %fusion.10 = f32[1024,2048]{1,0:T(8,128)} fusion(bf16[1024,1408]{1,0:T(8,128)(2,1)} %add_convert_fusion.1, bf16[2048,1408]{1,0:T(8,128)(2,1)} %all-gather.4.cloned.1.call-done), kind=kOutput, calls=%fused_computation.30 | convolution fusion | flops 5905580032 | bytes 17039360 | tf_op jit(solution)/shard_map/dot_general | solution.py:14
  152.9 81.1 %all-gather.6.cloned.1.call-done = bf16[2048,1408]{1,0:T(8,128)(2,1)} async-done(((bf16[256,1408]{1,0:T(8,128)(2,1)}), bf16[2048,1408]{1,0:T(8,128)(2,1)}) %all-gather.6.cloned.1.call-update) | async-done | bytes 5767184 | tf_op jit(solution)/shard_map/all_gather | solution.py:55
  234.0 13.6 %add_convert_fusion = bf16[1024,2048]{1,0:T(8,128)(2,1)} fusion(f32[1024,2048]{1,0:T(8,128)} %fusion.10, bf16[2048,1408]{1,0:T(8,128)(2,1)} %all-gather.6.cloned.1.call-done, bf16[1024,1408]{1,0:T(8,128)(2,1)S(1)} %copy-done.3, f32[1024,1408]{1,0:T(8,128)} %get-tuple-element.18), kind=kOutput, calls=%fused_computation.3 | convolution fusion | flops 5925634048 | bytes 27000832 | tf_op jit(solution)/shard_map/dot_general | solution.py:14
  247.7 36.5 %psum.7 = f32[4,1408]{1,0:T(4,128)S(1)} all-reduce(f32[4,1408]{1,0:T(4,128)S(1)} %pad_maximum_fusion.1), channel_id=1, replica_groups=mesh['fs'=8,'tp'=4] {'fs'}, use_global_device_ids=true, to_apply=%region_6.7 | all-reduce | flops 5632 | bytes 45056 | tf_op jit(solution)/shard_map/psum | solution.py:51
  284.2 0.6 slice_reduce_fusion
  284.8 325.4 %reduce-scatter.5.cloned.1.call-done = f32[256,2816]{0,1:T(8,128)} async-done(((f32[2048,2816]{0,1:T(8,128)}), f32[256,2816]{0,1:T(8,128)}) %reduce-scatter.5.cloned.1.call-update) | async-done | bytes 2883600 | tf_op jit(solution)/shard_map/reduce_scatter | solution.py:57
  610.2 2.0 slice_multiply_fusion
  612.3 1.5 copy.14
  613.8 1.5 copy.13
  615.4 41.6 %reduce-scatter.3.cloned.1.call-done = bf16[256,2048]{1,0:T(8,128)(2,1)} async-done(((bf16[1024,2048]{1,0:T(8,128)(2,1)}), bf16[256,2048]{1,0:T(8,128)(2,1)}) %reduce-scatter.3.cloned.1.call-update) | async-done | bytes 1048592 | tf_op jit(solution)/shard_map/reduce_scatter | solution.py:68
  (25 shorter events, 0.3 us)
Async XLA Ops:
  7.2 4.7 copy-start
  7.2 4.7 copy-start.5
  7.2 4.7 copy-start.6
  7.2 39.6 %all-gather.8.cloned.1.call-start = ((), (), s32[]{:S(2)}) async-start(), calls=%async_computation.5 | async-start | bytes 5242880 | tf_op jit(solution)/shard_map/all_gather | solution.py:52
  7.9 133.4 %all-gather.4.cloned.1.call-start = ((), (), s32[]{:S(2)}) async-start(), calls=%async_computation.2 | async-start | bytes 6488064 | tf_op jit(solution)/shard_map/all_gather | solution.py:54
  8.7 225.3 %all-gather.6.cloned.1.call-start = ((), (), s32[]{:S(2)}) async-start(), calls=%async_computation.3 | async-start | bytes 6488064 | tf_op jit(solution)/shard_map/all_gather | solution.py:55
  9.4 600.8 %reduce-scatter.5.cloned.1.call-start = ((), (), s32[]{:S(2)}) async-start(), calls=%async_computation.6 | async-start | bytes 25952256 | tf_op jit(solution)/shard_map/reduce_scatter | solution.py:57
  9.5 2.7 copy-start.1
  9.5 3.5 copy-start.2
  22.3 24.5 %copy-start.3 = (bf16[1024,1408]{1,0:T(8,128)(2,1)S(1)}, bf16[1024,1408]{1,0:T(8,128)(2,1)}, u32[]{:S(2)}) copy-start(bf16[1024,1408]{1,0:T(8,128)(2,1)} %param.15) | copy-start | bytes 8650756
  79.8 577.1 %reduce-scatter.3.cloned.1.call-start = ((), (), s32[]{:S(2)}) async-start(), calls=%async_computation.4 | async-start | bytes 5242880 | tf_op jit(solution)/shard_map/reduce_scatter | solution.py:68
  284.2 331.2 %copy-start.4 = (f32[4,1408]{1,0:T(4,128)}, f32[4,1408]{1,0:T(4,128)S(1)}, u32[]{:S(2)}) copy-start(f32[4,1408]{1,0:T(4,128)S(1)} %broadcast_multiply_fusion) | copy-start | bytes 67588
Sparse Core Ops, SparseCore 0:
  9.6 37.1 all-gather.7
  49.0 92.2 all-gather.3
  143.5 90.4 all-gather.5
  237.8 372.4 reduce-scatter.4
  613.2 43.6 reduce-scatter.2
where the time goes:
time: 664 us; the launch traced here: 663 us
  waiting for transfers between devices  533 us (80%)
  matrix products  46.9 us (7%)
  blocking collectives  36.5 us (5%)
  other arithmetic  28 us (4%)
  between operations  13.9 us (2%)
    reduce_scatter x1, waiting for transfers between devices, on_device(): lax.psum_scatter(jnp.concatenate([contract_rows(whole_tokens, gate_grad),...  325 us
    all_gather x1, waiting for transfers between devices, on_device(): lax.all_gather(up_value_w, 'fs', axis=0, tiled=True)  81.1 us
    all_gather x1, waiting for transfers between devices, on_device(): lax.all_gather(up_gate_w, 'fs', axis=0, tiled=True)  61.2 us
    reduce_scatter x1, waiting for transfers between devices, on_device(): lax.psum_scatter((contract_cols(gate_grad, full_gate) + contract_cols(val...  41.6 us
    psum x1, blocking collectives, on_device(): conv_total = lax.psum(conv_terms, 'fs') * scale  36.5 us
    dot_general x2, matrix products, contract_cols(): lax.dot_general(left, right, (((1,), (1,)), ((), ())), preferred_element_...  25.2 us
    dot_general x2, matrix products, contract_rows(): lax.dot_general(left, right, (((0,), (0,)), ((), ())), preferred_element_...  21.7 us
    all_gather x1, waiting for transfers between devices, on_device(): whole_tokens = lax.all_gather(tokens, 'tp', axis=0, tiled=True)  21.5 us
  transfers between devices with their start and end apart: 5, of which 5 were waited for; matrix products, arithmetic and copies ran while one was open for 12% of the time, Pallas kernels for 0%

commit v1 on v0

--- a/solution.py
+++ b/solution.py
@@ -14,6 +14,42 @@
     return lax.dot_general(
         left, right, (((1,), (1,)), ((), ())), preferred_element_type=jnp.float32
     )
+
+
+def ring_of(count):
+    return [*range(0, count, 2), *reversed(range(1, count, 2))]
+
+
+def ring_gather(block, axis, backward, tie_step, tie):
+    count = lax.axis_size(axis)
+    ring = ring_of(count)
+    if backward:
+        ring = ring[::-1]
+    hops = [(ring[i], ring[(i + 1) % count]) for i in range(count)]
+    place = [ring.index(i) for i in range(count)]
+    mine = jnp.asarray(place, jnp.int32)[lax.axis_index(axis)]
+    order = jnp.asarray(ring, jnp.int32)
+    rows = block.shape[0]
+    whole = jnp.zeros((rows * count, block.shape[1]), block.dtype)
+    for step in range(count):
+        owner = order[(mine - step + count) % count]
+        whole = lax.dynamic_update_slice(whole, block, (owner * rows, 0))
+        if step < count - 1:
+            if step == tie_step:
+                block, tie = lax.optimization_barrier((block, tie))
+            block = lax.ppermute(block, axis, hops)
+    return whole
+
+
+def sum_over(terms, axis):
+    count = lax.axis_size(axis)
+    if count & (count - 1):
+        return lax.psum(terms, axis)
+    reach = 1
+    while reach < count:
+        terms = terms + lax.ppermute(terms, axis, [(i, i ^ reach) for i in range(count)])
+        reach *= 2
+    return terms
 
 
 def on_device(
@@ -48,23 +84,23 @@
             jnp.sum(conv_grad, axis=0),
         ]
     )
-    conv_total = lax.psum(conv_terms, "fs") * scale
+    conv_total = sum_over(conv_terms, "fs") * scale
     whole_tokens = lax.all_gather(tokens, "tp", axis=0, tiled=True)
-    full_gate, full_value = (
-        lax.all_gather(up_gate_w, "fs", axis=0, tiled=True),
-        lax.all_gather(up_value_w, "fs", axis=0, tiled=True),
+    terms = [
+        contract_rows(whole_tokens, grad).astype(jnp.bfloat16) for grad in (gate_grad, value_grad)
+    ]
+    full_gate = ring_gather(up_gate_w, "fs", False, 3, terms[0][:1, :1])
+    full_value = ring_gather(up_value_w, "fs", True, 3, terms[0][:1, :1])
+    gate_out, value_out = (
+        lax.psum_scatter(
+            term,
+            "fs",
+            scatter_dimension=0,
+            tiled=True,
+        ).astype(jnp.float32)
+        * scale
+        for term in terms
     )
-    joined = lax.psum_scatter(
-        jnp.concatenate(
-            [contract_rows(whole_tokens, gate_grad), contract_rows(whole_tokens, value_grad)],
-            axis=1,
-        ),
-        "fs",
-        scatter_dimension=0,
-        tiled=True,
-    )
-    gate_out = joined[:, :col_count] * scale
-    value_out = joined[:, col_count:] * scale
     input_grad = lax.psum_scatter(
         (contract_cols(gate_grad, full_gate) + contract_cols(value_grad, full_value)).astype(
             jnp.bfloat16

time: 664 us -> 427 us (0.64)
  waiting for transfers between devices: 533 us -> 268 us
  starting transfers between devices: 0.37 us -> 42.9 us
  blocking collectives: 36.5 us -> 0 us
  between operations: 13.9 us -> 35.1 us
  local copies, waits for them, and re-layouts: 4.91 us -> 17.2 us
  other arithmetic: 28 us -> 16.1 us
    reduce_scatter x1 -> x2, waiting for transfers between devices: 325 us -> 12.9 us  [on_device(): lax.psum_scatter(term, 'fs', scatter_dimension=0, tiled=True)]
    ppermute x0 -> x17, waiting for transfers between devices: none -> 188 us  [the longest x14 178 us: ring_gather(): block = lax.ppermute(block, axis, hops)]
    all_gather x2 -> x0, waiting for transfers between devices: 142 us -> none  [the longest x1 81.1 us: on_device(): lax.all_gather(up_value_w, 'fs', axis=0, tiled=True)]
    ppermute x0 -> x17, starting transfers between devices: none -> 42.7 us  [the longest x14 37.1 us: ring_gather(): block = lax.ppermute(block, axis, hops)]
    psum x1 -> x0, blocking collectives: 36.5 us -> none  [on_device(): conv_total = lax.psum(conv_terms, 'fs') * scale]
    concatenate x1 -> x0, other arithmetic: 11.3 us -> none  [on_device(): jnp.concatenate([contract_rows(whole_tokens, gate_grad), contract_rows(wh...]
  transfers between devices with their start and end apart: 5 -> 21, of which waited for: 5 -> 14; matrix products, arithmetic and copies ran while one was open for 12% -> 15% of each run, Pallas kernels for 0% -> 0%
where the time goes in v1:
time: 427 us; the launch traced here: 426 us
  waiting for transfers between devices  268 us (63%)
  matrix products  46.7 us (11%)
  starting transfers between devices  42.9 us (10%)
  between operations  35.1 us (8%)
  local copies, waits for them, and re-layouts  17.2 us (4%)
  other arithmetic  16.1 us (4%)
    ppermute x14, waiting for transfers between devices, ring_gather(): block = lax.ppermute(block, axis, hops)  178 us
    reduce_scatter x1, waiting for transfers between devices, on_device(): lax.psum_scatter((contract_cols(gate_grad, full_gate) + contract_cols(val...  43.4 us
    ppermute x14, starting transfers between devices, ring_gather(): block = lax.ppermute(block, axis, hops)  37.1 us
    dot_general x2, matrix products, contract_rows(): lax.dot_general(left, right, (((0,), (0,)), ((), ())), preferred_element_...  24.9 us
    all_gather x1, waiting for transfers between devices, on_device(): whole_tokens = lax.all_gather(tokens, 'tp', axis=0, tiled=True)  23.8 us
    dot_general x2, matrix products, contract_cols(): lax.dot_general(left, right, (((1,), (1,)), ((), ())), preferred_element_...  21.8 us
    reduce_scatter x2, waiting for transfers between devices, on_device(): lax.psum_scatter(term, 'fs', scatter_dimension=0, tiled=True)  12.9 us
    ppermute x3, waiting for transfers between devices, sum_over(): lax.ppermute(terms, axis, [(i, i ^ reach) for i in range(count)])  9.79 us
  transfers between devices with their start and end apart: 21, of which 14 were waited for; matrix products, arithmetic and copies ran while one was open for 15% of the time, Pallas kernels for 0%

profile of v1, /device:TPU:0, one launch (start us, length us, event | category | flops | bytes accessed | tf_op | source)
XLA Modules:
  0.0 426.4 jit_solution(921284441572140730)
XLA Ops:
  8.0 2.3 convert_element_type.42
  11.8 9.3 %multiply_reduce_fusion.2 = (f32[1408]{0:T(1024)S(1)}, f32[1408]{0:T(1024)S(1)}, f32[1408]{0:T(1024)S(1)}, f32[1408]{0:T(1024)S(1)}, f32[1024,1408]{1,0:T(8,128)S(1)}, /*index=5*/f32[1024,1408]{1,0:T(8,128)}) fusion(f32[1024,1408]{1,0:T(8,128)S(1)} %convert_element_type.42, bf16[1024,1408]{1,0:T(8,128)(2,1)S(1)} %copy-done, ...), kind=kLoop, calls=%fused_computation.18 | loop fusion | flops 51898880 | bytes 25997312 | tf_op jit(solution)/shard_map/reduce_sum | solution.py:81
  23.0 23.8 %all-gather.2.cloned.1.call-done = bf16[1024,2048]{1,0:T(8,128)(2,1)} async-done(((bf16[256,2048]{1,0:T(8,128)(2,1)}), bf16[1024,2048]{1,0:T(8,128)(2,1)}) %all-gather.2.cloned.1.call-update) | async-done | bytes 4194320 | tf_op jit(solution)/shard_map/all_gather | solution.py:88
  46.8 10.8 %fusion = bf16[2048,1408]{0,1:T(8,128)(2,1)} fusion(bf16[1024,1408]{1,0:T(8,128)(2,1)S(1)} %add_convert_fusion.1, bf16[1024,2048]{1,0:T(8,128)(2,1)} %all-gather.2.cloned.1.call-done), kind=kOutput, calls=%fused_computation.7 | convolution fusion | flops 5908463616 | bytes 12845056 | tf_op jit(solution)/shard_map/dot_general | solution.py:8
  59.4 14.2 %fusion.1 = bf16[2048,1408]{0,1:T(8,128)(2,1)} fusion(bf16[1024,2048]{1,0:T(8,128)(2,1)} %all-gather.2.cloned.1.call-done, bf16[1024,1408]{1,0:T(8,128)(2,1)S(1)} %copy-done.3, f32[1024,1408]{1,0:T(8,128)} %get-tuple-element.22), kind=kOutput, calls=%fused_computation.8 | convolution fusion | flops 5924323328 | bytes 18612224 | tf_op jit(solution)/shard_map/dot_general | solution.py:8
  75.7 31.6 %collective-permute-done = bf16[256,1408]{1,0:T(8,128)(2,1)S(1)} collective-permute-done((bf16[256,1408]{1,0:T(8,128)(2,1)}, bf16[256,1408]{1,0:T(8,128)(2,1)S(1)}, u32[]{:S(2)}, u32[]{:S(2)}) %collective-permute-start) | collective-permute-done | bytes 720928 | tf_op jit(solution)/shard_map/ppermute | solution.py:40
  108.1 10.8 %collective-permute-start.1 = (bf16[256,1408]{1,0:T(8,128)(2,1)S(1)}, bf16[256,1408]{1,0:T(8,128)(2,1)}, u32[]{:S(2)}, u32[]{:S(2)}) collective-permute-start(bf16[256,1408]{1,0:T(8,128)(2,1)S(1)} %collective-permute-done), channel_id=1, source_target_pairs={{0,8},{8,16},{16,24},{24,28},{28,20},{20,12},{12,4},{4,0},{1,9},{9... | collective-permute-start | bytes 2162696 | tf_op jit(solution)/shard_map/ppermute | solution.py:40
  122.7 23.2 %collective-permute-done.1 = bf16[256,1408]{1,0:T(8,128)(2,1)} collective-permute-done((bf16[256,1408]{1,0:T(8,128)(2,1)S(1)}, bf16[256,1408]{1,0:T(8,128)(2,1)}, u32[]{:S(2)}, u32[]{:S(2)}) %collective-permute-start.1) | collective-permute-done | bytes 720928 | tf_op jit(solution)/shard_map/ppermute | solution.py:40
  173.8 30.5 %collective-permute-done.9 = bf16[256,1408]{1,0:T(8,128)(2,1)S(1)} collective-permute-done((bf16[256,1408]{1,0:T(8,128)(2,1)}, bf16[256,1408]{1,0:T(8,128)(2,1)S(1)}, u32[]{:S(2)}, u32[]{:S(2)}) %collective-permute-start.9) | collective-permute-done | bytes 720928 | tf_op jit(solution)/shard_map/ppermute | solution.py:40
  205.6 9.1 %collective-permute-start.4 = (bf16[256,1408]{1,0:T(8,128)(2,1)S(1)}, bf16[256,1408]{1,0:T(8,128)(2,1)S(1)}, u32[]{:S(2)}, u32[]{:S(2)}) collective-permute-start(bf16[256,1408]{1,0:T(8,128)(2,1)S(1)} %collective-permute-done.3), channel_id=1, source_target_pairs={{0,8},{8,16},{16,24},{24,28},{28,20},{20,12},{12,4},{4,0},{1,9},{9... | collective-permute-start | bytes 2162696 | tf_op jit(solution)/shard_map/ppermute | solution.py:40
  216.0 8.8 %collective-permute-done.10 = bf16[256,1408]{1,0:T(8,128)(2,1)S(1)} collective-permute-done((bf16[256,1408]{1,0:T(8,128)(2,1)S(1)}, bf16[256,1408]{1,0:T(8,128)(2,1)S(1)}, u32[]{:S(2)}, u32[]{:S(2)}) %collective-permute-start.10) | collective-permute-done | bytes 720928 | tf_op jit(solution)/shard_map/ppermute | solution.py:40
  226.4 2.8 collective-permute-start.5
  229.3 32.6 %collective-permute-done.11 = bf16[256,1408]{1,0:T(8,128)(2,1)S(1)} collective-permute-done((bf16[256,1408]{1,0:T(8,128)(2,1)S(1)}, bf16[256,1408]{1,0:T(8,128)(2,1)S(1)}, u32[]{:S(2)}, u32[]{:S(2)}) %collective-permute-start.11) | collective-permute-done | bytes 720928 | tf_op jit(solution)/shard_map/ppermute | solution.py:40
  262.1 8.2 %collective-permute-start.6 = (bf16[256,1408]{1,0:T(8,128)(2,1)S(1)}, bf16[256,1408]{1,0:T(8,128)(2,1)S(1)}, u32[]{:S(2)}, u32[]{:S(2)}) collective-permute-start(bf16[256,1408]{1,0:T(8,128)(2,1)S(1)} %collective-permute-done.5), channel_id=1, source_target_pairs={{0,8},{8,16},{16,24},{24,28},{28,20},{20,12},{12,4},{4,0},{1,9},{9... | collective-permute-start | bytes 2162696 | tf_op jit(solution)/shard_map/ppermute | solution.py:40
  270.4 28.3 %collective-permute-done.12 = bf16[256,1408]{1,0:T(8,128)(2,1)S(1)} collective-permute-done((bf16[256,1408]{1,0:T(8,128)(2,1)S(1)}, bf16[256,1408]{1,0:T(8,128)(2,1)S(1)}, u32[]{:S(2)}, u32[]{:S(2)}) %collective-permute-start.12) | collective-permute-done | bytes 720928 | tf_op jit(solution)/shard_map/ppermute | solution.py:40
  299.0 20.9 %collective-permute-done.13 = bf16[256,1408]{1,0:T(8,128)(2,1)S(1)} collective-permute-done((bf16[256,1408]{1,0:T(8,128)(2,1)S(1)}, bf16[256,1408]{1,0:T(8,128)(2,1)S(1)}, u32[]{:S(2)}, u32[]{:S(2)}) %collective-permute-start.13) | collective-permute-done | bytes 720928 | tf_op jit(solution)/shard_map/ppermute | solution.py:40
  320.0 10.3 %fusion.11 = f32[1024,2048]{1,0:T(8,128)} fusion(bf16[2048,1408]{1,0:T(8,128)(2,1)S(1)} %constant_dynamic-update-slice_fusion, bf16[1024,1408]{1,0:T(8,128)(2,1)S(1)} %copy-done.3, f32[1024,1408]{1,0:T(8,128)S(1)} %bitcast.44), kind=kOutput, calls=%fused_computation.48 | convolution fusion | flops 5921439744 | bytes 22806528 | tf_op jit(solution)/shard_map/dot_general | solution.py:14
  330.4 11.5 %add_convert_fusion = bf16[1024,2048]{1,0:T(8,128)(2,1)} fusion(f32[1024,2048]{1,0:T(8,128)} %fusion.11, bf16[1024,1408]{1,0:T(8,128)(2,1)} %copy-done.4, bf16[2048,1408]{1,0:T(8,128)(2,1)S(1)} %constant_dynamic-update-slice_fusion.8), kind=kOutput, calls=%fused_computation | convolution fusion | flops 5909774336 | bytes 21233664 | tf_op jit(solution)/shard_map/dot_general | solution.py:14
  342.0 3.8 collective-permute-done.14
  348.1 2.4 collective-permute-done.15
  350.5 3.3 collective-permute-start.16
  353.8 3.6 collective-permute-done.16
  360.8 12.9 %reduce-scatter.8.cloned.1.call-done = bf16[256,1408]{0,1:T(8,128)(2,1)} async-done(((bf16[2048,1408]{0,1:T(8,128)(2,1)}), bf16[256,1408]{0,1:T(8,128)(2,1)}) %reduce-scatter.8.cloned.1.call-update) | async-done | bytes 720912 | tf_op jit(solution)/shard_map/reduce_scatter | solution.py:95
  376.5 43.4 %reduce-scatter.4.cloned.1.call-done = bf16[256,2048]{1,0:T(8,128)(2,1)} async-done(((bf16[1024,2048]{1,0:T(8,128)(2,1)}), bf16[256,2048]{1,0:T(8,128)(2,1)}) %reduce-scatter.4.cloned.1.call-update) | async-done | bytes 1048592 | tf_op jit(solution)/shard_map/reduce_scatter | solution.py:104
  (102 shorter events, 33.1 us)
Async XLA Ops:
  7.2 39.6 %all-gather.2.cloned.1.call-start = ((), (), s32[]{:S(2)}) async-start(), calls=%async_computation.3 | async-start | bytes 5242880 | tf_op jit(solution)/shard_map/all_gather | solution.py:88
  7.9 350.1 %reduce-scatter.6.cloned.1.call-start = ((), (), s32[]{:S(2)}) async-start(), calls=%async_computation.5 | async-start | bytes 6488064 | tf_op jit(solution)/shard_map/reduce_scatter | solution.py:95
  57.6 316.2 %reduce-scatter.8.cloned.1.call-start = ((), (), s32[]{:S(2)}) async-start(), calls=%async_computation.6 | async-start | bytes 6488064 | tf_op jit(solution)/shard_map/reduce_scatter | solution.py:95
  73.5 84.2 %copy-start.11 = (s32[8]{0:T(128)S(1)}, s32[8]{0:T(128)}, u32[]{:S(2)}) copy-start(s32[8]{0:T(128)} %constant.188.clone) | copy-start | bytes 100
  73.5 90.0 %copy-start.10 = (s32[8]{0:T(128)S(1)}, s32[8]{0:T(128)}, u32[]{:S(2)}) copy-start(s32[8]{0:T(128)} %constant.190.clone) | copy-start | bytes 100
  73.6 346.3 %reduce-scatter.4.cloned.1.call-start = ((), (), s32[]{:S(2)}) async-start(), calls=%async_computation.4 | async-start | bytes 5242880 | tf_op jit(solution)/shard_map/reduce_scatter | solution.py:104
  73.6 33.7 %collective-permute-start = (bf16[256,1408]{1,0:T(8,128)(2,1)}, bf16[256,1408]{1,0:T(8,128)(2,1)S(1)}, u32[]{:S(2)}, u32[]{:S(2)}) collective-permute-start(bf16[256,1408]{1,0:T(8,128)(2,1)} %param.15), channel_id=1, source_target_pairs={{0,8},{8,16},{16,24},{24,28},{28,20},{20,12},{12,4},{4,0},{1,9},{9... | collective-permute-start | bytes 2162696 | tf_op jit(solution)/shard_map/ppermute | solution.py:40
  75.2 45.7 %collective-permute-start.7 = (bf16[256,1408]{1,0:T(8,128)(2,1)}, bf16[256,1408]{1,0:T(8,128)(2,1)}, u32[]{:S(2)}, u32[]{:S(2)}) collective-permute-start(bf16[256,1408]{1,0:T(8,128)(2,1)} %param.16), channel_id=1, source_target_pairs={{4,12},{12,20},{20,28},{28,24},{24,16},{16,8},{8,0},{0,4},{5,13},{... | collective-permute-start | bytes 2162696 | tf_op jit(solution)/shard_map/ppermute | solution.py:40
  108.1 37.7 %collective-permute-start.1 = (bf16[256,1408]{1,0:T(8,128)(2,1)S(1)}, bf16[256,1408]{1,0:T(8,128)(2,1)}, u32[]{:S(2)}, u32[]{:S(2)}) collective-permute-start(bf16[256,1408]{1,0:T(8,128)(2,1)S(1)} %collective-permute-done), channel_id=1, source_target_pairs={{0,8},{8,16},{16,24},{24,28},{28,20},{20,12},{12,4},{4,0},{1,9},{9... | collective-permute-start | bytes 2162696 | tf_op jit(solution)/shard_map/ppermute | solution.py:40
  120.9 48.5 %collective-permute-start.8 = (bf16[256,1408]{1,0:T(8,128)(2,1)}, bf16[256,1408]{1,0:T(8,128)(2,1)}, u32[]{:S(2)}, u32[]{:S(2)}) collective-permute-start(bf16[256,1408]{1,0:T(8,128)(2,1)} %collective-permute-done.7), channel_id=1, source_target_pairs={{4,12},{12,20},{20,28},{28,24},{24,16},{16,8},{8,0},{0,4},{5,13},{... | collective-permute-start | bytes 2162696 | tf_op jit(solution)/shard_map/ppermute | solution.py:40
  145.9 26.6 %collective-permute-start.2 = (bf16[256,1408]{1,0:T(8,128)(2,1)}, bf16[256,1408]{1,0:T(8,128)(2,1)}, u32[]{:S(2)}, u32[]{:S(2)}) collective-permute-start(bf16[256,1408]{1,0:T(8,128)(2,1)} %collective-permute-done.1), channel_id=1, source_target_pairs={{0,8},{8,16},{16,24},{24,28},{28,20},{20,12},{12,4},{4,0},{1,9},{9... | collective-permute-start | bytes 2162696 | tf_op jit(solution)/shard_map/ppermute | solution.py:40
  169.4 34.9 %collective-permute-start.9 = (bf16[256,1408]{1,0:T(8,128)(2,1)}, bf16[256,1408]{1,0:T(8,128)(2,1)S(1)}, u32[]{:S(2)}, u32[]{:S(2)}) collective-permute-start(bf16[256,1408]{1,0:T(8,128)(2,1)} %collective-permute-done.8), channel_id=1, source_target_pairs={{4,12},{12,20},{20,28},{28,24},{24,16},{16,8},{8,0},{0,4},{5,13},{... | collective-permute-start | bytes 2162696 | tf_op jit(solution)/shard_map/ppermute | solution.py:40
  172.5 33.0 %collective-permute-start.3 = (bf16[256,1408]{1,0:T(8,128)(2,1)}, bf16[256,1408]{1,0:T(8,128)(2,1)S(1)}, u32[]{:S(2)}, u32[]{:S(2)}) collective-permute-start(bf16[256,1408]{1,0:T(8,128)(2,1)} %collective-permute-done.2), channel_id=1, source_target_pairs={{0,8},{8,16},{16,24},{24,28},{28,20},{20,12},{12,4},{4,0},{1,9},{9... | collective-permute-start | bytes 2162696 | tf_op jit(solution)/shard_map/ppermute | solution.py:40
  204.3 20.6 %collective-permute-start.10 = (bf16[256,1408]{1,0:T(8,128)(2,1)S(1)}, bf16[256,1408]{1,0:T(8,128)(2,1)S(1)}, u32[]{:S(2)}, u32[]{:S(2)}) collective-permute-start(bf16[256,1408]{1,0:T(8,128)(2,1)S(1)} %collective-permute-done.9), channel_id=1, source_target_pairs={{4,12},{12,20},{20,28},{28,24},{24,16},{16,8},{8,0},{0,4},{5,13},{... | collective-permute-start | bytes 2162696 | tf_op jit(solution)/shard_map/ppermute | solution.py:40
  205.6 20.8 %collective-permute-start.4 = (bf16[256,1408]{1,0:T(8,128)(2,1)S(1)}, bf16[256,1408]{1,0:T(8,128)(2,1)S(1)}, u32[]{:S(2)}, u32[]{:S(2)}) collective-permute-start(bf16[256,1408]{1,0:T(8,128)(2,1)S(1)} %collective-permute-done.3), channel_id=1, source_target_pairs={{0,8},{8,16},{16,24},{24,28},{28,20},{20,12},{12,4},{4,0},{1,9},{9... | collective-permute-start | bytes 2162696 | tf_op jit(solution)/shard_map/ppermute | solution.py:40
  214.6 105.3 %slice-start = ((s8[5767168]{0:T(1024)(128)(4,1)}), s8[4194304]{0:T(1024)(128)(4,1)S(1)}, s32[]{:S(2)}) async-start(s8[5767168]{0:T(1024)(128)(4,1)} %bitcast.43), calls=%async_computation.7 | async-start | bytes 8388608
  224.8 37.0 %collective-permute-start.11 = (bf16[256,1408]{1,0:T(8,128)(2,1)S(1)}, bf16[256,1408]{1,0:T(8,128)(2,1)S(1)}, u32[]{:S(2)}, u32[]{:S(2)}) collective-permute-start(bf16[256,1408]{1,0:T(8,128)(2,1)S(1)} %collective-permute-done.10), channel_id=1, source_target_pairs={{4,12},{12,20},{20,28},{28,24},{24,16},{16,8},{8,0},{0,4},{5,13},{... | collective-permute-start | bytes 2162696 | tf_op jit(solution)/shard_map/ppermute | solution.py:40
  226.4 35.7 %collective-permute-start.5 = (bf16[256,1408]{1,0:T(8,128)(2,1)S(1)}, bf16[256,1408]{1,0:T(8,128)(2,1)S(1)}, u32[]{:S(2)}, u32[]{:S(2)}) collective-permute-start(bf16[256,1408]{1,0:T(8,128)(2,1)S(1)} %collective-permute-done.4), channel_id=1, source_target_pairs={{0,8},{8,16},{16,24},{24,28},{28,20},{20,12},{12,4},{4,0},{1,9},{9... | collective-permute-start | bytes 2162696 | tf_op jit(solution)/shard_map/ppermute | solution.py:40
  261.9 36.8 %collective-permute-start.12 = (bf16[256,1408]{1,0:T(8,128)(2,1)S(1)}, bf16[256,1408]{1,0:T(8,128)(2,1)S(1)}, u32[]{:S(2)}, u32[]{:S(2)}) collective-permute-start(bf16[256,1408]{1,0:T(8,128)(2,1)S(1)} %collective-permute-done.11), channel_id=1, source_target_pairs={{4,12},{12,20},{20,28},{28,24},{24,16},{16,8},{8,0},{0,4},{5,13},{... | collective-permute-start | bytes 2162696 | tf_op jit(solution)/shard_map/ppermute | solution.py:40
  262.1 36.8 %collective-permute-start.6 = (bf16[256,1408]{1,0:T(8,128)(2,1)S(1)}, bf16[256,1408]{1,0:T(8,128)(2,1)S(1)}, u32[]{:S(2)}, u32[]{:S(2)}) collective-permute-start(bf16[256,1408]{1,0:T(8,128)(2,1)S(1)} %collective-permute-done.5), channel_id=1, source_target_pairs={{0,8},{8,16},{16,24},{24,28},{28,20},{20,12},{12,4},{4,0},{1,9},{9... | collective-permute-start | bytes 2162696 | tf_op jit(solution)/shard_map/ppermute | solution.py:40
  298.7 21.2 %collective-permute-start.13 = (bf16[256,1408]{1,0:T(8,128)(2,1)S(1)}, bf16[256,1408]{1,0:T(8,128)(2,1)S(1)}, u32[]{:S(2)}, u32[]{:S(2)}) collective-permute-start(bf16[256,1408]{1,0:T(8,128)(2,1)S(1)} %collective-permute-done.12), channel_id=1, source_target_pairs={{4,12},{12,20},{20,28},{28,24},{24,16},{16,8},{8,0},{0,4},{5,13},{... | collective-permute-start | bytes 2162696 | tf_op jit(solution)/shard_map/ppermute | solution.py:40
  341.9 3.9 collective-permute-start.14
  345.8 4.7 %collective-permute-start.15 = (f32[4,1408]{1,0:T(4,128)S(1)}, f32[4,1408]{1,0:T(4,128)S(1)}, u32[]{:S(2)}, u32[]{:S(2)}) collective-permute-start(f32[4,1408]{1,0:T(4,128)S(1)} %fusion.9), channel_id=1, source_target_pairs={{0,8},{4,12},{8,0},{12,4},{16,24},{20,28},{24,16},{28,20},{1,9},{5... | collective-permute-start | bytes 67592 | tf_op jit(solution)/shard_map/ppermute | solution.py:50
  350.5 6.9 %collective-permute-start.16 = (f32[4,1408]{1,0:T(4,128)S(1)}, f32[4,1408]{1,0:T(4,128)S(1)}, u32[]{:S(2)}, u32[]{:S(2)}) collective-permute-start(f32[4,1408]{1,0:T(4,128)S(1)} %fusion.22), channel_id=1, source_target_pairs={{0,16},{4,20},{8,24},{12,28},{16,0},{20,4},{24,8},{28,12},{1,17},{... | collective-permute-start | bytes 67592 | tf_op jit(solution)/shard_map/ppermute | solution.py:50
  (15 other events, 352.0 us)
Sparse Core Ops, SparseCore 0:
  9.6 37.1 all-gather.1
  57.7 158.1 reduce-scatter.5
  219.6 154.1 reduce-scatter.7
  376.7 43.1 reduce-scatter.3
